TPU v7x, 128 devices: a whole 4x4x4 slice. The times are simulated.
128 devices in a mesh: sp: 16 (over z, y), fs: 4 (over x), tp: 2 (over core).
Axes of the slice: x: 4, y: 4, z: 4, core: 2. Of those that a mesh axis runs over, the one named last changes fastest.
Arguments:
- tokens: bfloat16 [4, 32768, 2048], P('fs', 'sp'), may hold values from -21 to 21
- norm_gain: float32 [2048], replicated, may hold values from 0.1 to 1.9
- w_query: bfloat16 [2048, 1024], P(None, 'tp'), may hold values from -0.125 to 0.125
- w_key: bfloat16 [2048, 256], P(None, 'tp'), may hold values from -0.125 to 0.125
- w_value: bfloat16 [2048, 256], P(None, 'tp'), may hold values from -0.125 to 0.125
- w_pool: bfloat16 [2048, 1024], P(None, 'tp'), may hold values from -0.125 to 0.125
- w_group: bfloat16 [4, 256, 256], P('tp'), may hold values from -0.375 to 0.375
- w_out: bfloat16 [2048, 2048], replicated, may hold values from -0.125 to 0.125
- sinks: float32 [16], P('tp'), may hold values from -1 to 260
Outputs:
- mixed: bfloat16 [4, 32768, 2048], P('fs', ('sp', 'tp'))
- log_sums: float32 [4, 16, 32768], P('fs', 'tp', 'sp')
All inputs are finite; a program needn't handle non-finite values.
Results may differ from a plain program's by a relative error of at most 0.009.
Values may be sent and summed in bfloat16 or wider, within the bound.
A program may use at most 192 MiB of HBM per device.

v0:
```python
import functools

import jax
import jax.numpy as jnp
from jax import lax
from jax.experimental import pallas as pl
from jax.experimental.pallas import tpu as pltpu
from jax.sharding import PartitionSpec as P

HEAD_SIZE = 64
GROUPS = 4
GDIM = 256
WINDOW_KEYS = 128
QUERY_HEADS = 16
KEY_VALUE_HEADS = 4
LN_EPS = 1e-05

BLK = 128
HALO = 16
TILE = 256
F32, BF16 = jnp.float32, jnp.bfloat16


MESH = pl.DeviceIdType.MESH
PART = 4


def project_kernel(
    tok,
    gain,
    w_query,
    w_key,
    w_value,
    w_pool,
    w_group,
    sinks,
    X,
    WP,
    WQ,
    WKV,
    WG,
    SK,
    PA,
    QA,
    TA,
    GAIN,
    SINK,
    WPO,
    WQO,
    x_sem,
    w_sem,
    small_sem,
    send_sem,
    recv_sem,
):
    rows, width = X.shape
    blocks = rows // BLK
    half_k = WKV.shape[1] // 4
    own_heads = QUERY_HEADS // 2
    tp = lax.axis_index("tp")
    peer = {"tp": 1 - tp}

    barrier = pltpu.get_barrier_semaphore()
    pl.semaphore_signal(barrier, inc=1, device_id=peer, device_id_type=MESH)

    small = [
        pltpu.make_async_copy(gain, GAIN, small_sem.at[0]),
        pltpu.make_async_copy(sinks, SINK, small_sem.at[1]),
    ]
    for copy in small:
        copy.start()

    def x_copy(b):
        return pltpu.make_async_copy(
            tok.at[pl.ds(pl.multiple_of(tp * rows + b * BLK, BLK), BLK), :],
            X.at[pl.ds(pl.multiple_of(b * BLK, BLK), BLK), :],
            x_sem.at[b],
        )

    @pl.loop(0, blocks)
    def _(b):
        x_copy(b).start()

    own = [
        pltpu.make_async_copy(src, dst, w_sem.at[i])
        for i, (src, dst) in enumerate(
            (
                (w_pool, WPO),
                (w_query, WQO),
                (w_key, WKV.at[:, 0:half_k]),
                (w_value, WKV.at[:, 2 * half_k : 3 * half_k]),
                (w_group, WG.at[0 : GROUPS // 2]),
            )
        )
    ]
    for copy in own:
        copy.start()

    for copy in small:
        copy.wait()
    row_of = lax.broadcasted_iota(jnp.int32, (own_heads, 128), 0)
    sink_block = jnp.zeros((own_heads, 128), F32)
    for h in range(own_heads):
        sink_block = jnp.where(row_of == h, SINK[h], sink_block)
    SK[0:own_heads, :] = sink_block

    pl.semaphore_wait(barrier, 1)
    sends = [
        pltpu.make_async_remote_copy(
            src_ref=src,
            dst_ref=dst,
            send_sem=send_sem.at[i],
            recv_sem=recv_sem.at[i],
            device_id=peer,
            device_id_type=MESH,
        )
        for i, (src, dst) in enumerate(
            (
                (w_pool, WP),
                (w_key, WKV.at[:, half_k : 2 * half_k]),
                (w_value, WKV.at[:, 3 * half_k : 4 * half_k]),
                (w_query, WQ),
                (w_group, WG.at[GROUPS // 2 : GROUPS]),
                (SK.at[0:own_heads], SK.at[own_heads : 2 * own_heads]),
            )
        )
    ]
    for copy in sends:
        copy.start()

    gains = GAIN[...]

    @pl.loop(0, blocks)
    def _(b):
        x_copy(b).wait()
        at = pl.ds(pl.multiple_of(b * BLK, BLK), BLK)
        values = X[at, :].astype(F32)
        mean = jnp.sum(values, axis=-1, keepdims=True) * (1.0 / width)
        centered = values - mean
        variance = jnp.sum(centered * centered, axis=-1, keepdims=True) * (1.0 / width)
        X[at, :] = (centered * lax.rsqrt(variance + LN_EPS) * gains).astype(BF16)

    own[0].wait()
    tile = jnp.dot(X[...], WPO[...], preferred_element_type=F32).astype(BF16)
    PA[...] = tile
    TA[...] = jnp.sum(tile.astype(F32), axis=0, keepdims=True)
    own[1].wait()
    tile = jnp.dot(X[...], WQO[...], preferred_element_type=F32) * (HEAD_SIZE**-0.5)
    QA[...] = tile.astype(BF16).T

    for copy in own[2:]:
        copy.wait()
    for copy in sends:
        copy.wait()


def mixer_kernel(
    sp_count,
    X,
    WP,
    WQ,
    WKV,
    WG,
    SK,
    PA,
    QA,
    TA,
    ACT,
    LSR,
    PB,
    QB,
    KB,
    VT,
    PH,
    KH,
    VH,
    LS,
    TOT,
    EARLIER,
    RECV,
    BAND,
    hsend_sem,
    hrecv_sem,
    tsend_sem,
    trecv_sem,
    lsend_sem,
    lrecv_sem,
):
    rows, kw = KB.shape
    half_p, half_q, half_k = PA.shape[1], QA.shape[0], kw // 2
    pw, qw = 2 * half_p, 2 * half_q
    blocks = rows // BLK
    sp, tp = lax.axis_index("sp"), lax.axis_index("tp")
    me = sp * 2 + tp
    count = sp_count * 2
    own_heads = QUERY_HEADS // 2
    first, last = me == 0, me == count - 1

    def mesh_id(index):
        return {"sp": index // 2, "tp": lax.rem(index, 2)}

    barrier = pltpu.get_barrier_semaphore()

    @pl.loop(1, count)
    def _(step):
        pl.semaphore_signal(
            barrier,
            inc=1,
            device_id=mesh_id(lax.rem(me + step, count)),
            device_id_type=MESH,
        )

    @pl.when(first)
    def _():
        PH[...] = jnp.zeros_like(PH)
        KH[...] = jnp.zeros_like(KH)
        VH[...] = jnp.zeros_like(VH)

    tile = jnp.dot(X[...], WP[...], preferred_element_type=F32).astype(BF16)
    PB[...] = tile
    TOT[pl.ds(tp, 1), 0] = TA[...]
    TOT[pl.ds(1 - tp, 1), 0] = jnp.sum(tile.astype(F32), axis=0, keepdims=True)
    tile = jnp.dot(X[...], WKV[...], preferred_element_type=F32).astype(BF16)
    KB[...] = tile[:, :kw]
    VT[...] = tile[:, kw:].T
    tile = jnp.dot(X[...], WQ[...], preferred_element_type=F32) * (HEAD_SIZE**-0.5)
    QB[...] = tile.astype(BF16).T

    tail, own_k, other_k = slice(rows - BLK, rows), slice(0, half_k), slice(half_k, kw)
    halo_copies = [
        pltpu.make_async_remote_copy(
            src_ref=src,
            dst_ref=dst,
            send_sem=hsend_sem.at[i],
            recv_sem=hrecv_sem.at[i],
            device_id=mesh_id(lax.rem(me + 1, count)),
            device_id_type=MESH,
        )
        for i, (src, dst) in enumerate(
            (
                (KB.at[tail, own_k], KH.at[:, other_k]),
                (KB.at[tail, other_k], KH.at[:, own_k]),
                (VT.at[own_k, tail], VH.at[other_k, :]),
                (VT.at[other_k, tail], VH.at[own_k, :]),
                (PA.at[rows - HALO : rows], PH.at[1]),
                (PB.at[rows - HALO : rows], PH.at[0]),
            )
        )
    ]

    def total_copy(target, slot):
        return pltpu.make_async_remote_copy(
            src_ref=TOT,
            dst_ref=RECV.at[me],
            send_sem=tsend_sem.at[slot],
            recv_sem=trecv_sem.at[me],
            device_id=mesh_id(target),
            device_id_type=MESH,
        )

    pl.semaphore_wait(barrier, count - 1)

    @pl.when(jnp.logical_not(last))
    def _():
        for copy in halo_copies:
            copy.start()

    @pl.loop(1, count)
    def _(step):
        @pl.when(me + step < count)
        def _():
            total_copy(me + step, step).start()

    span = HALO + BLK
    pairs = 2 * BLK
    older = lax.broadcasted_iota(jnp.int32, (BLK, pairs), 0) > (
        lax.broadcasted_iota(jnp.int32, (BLK, pairs), 1) & (BLK - 1)
    )
    back = (
        lax.broadcasted_iota(jnp.int32, (BLK, span), 0)
        + HALO
        - lax.broadcasted_iota(jnp.int32, (BLK, span), 1)
    )
    in_block = lax.broadcasted_iota(jnp.int32, (BLK, span), 1) >= HALO
    prefix_ones = jnp.where((back >= 0) & in_block, 1.0, 0.0).astype(BF16)
    groups = [lax.rem(2 * tp + j, GROUPS) for j in range(GROUPS)]
    reaches = [jnp.left_shift(jnp.int32(2), group) for group in groups]
    for j, reach in enumerate(reaches):
        BAND[j, 0:BLK, :] = jnp.where(
            (back >= 0) & (back < reach), 1.0 / reach.astype(F32), 0.0
        ).astype(BF16)
        BAND[j, BLK : 2 * BLK, :] = prefix_ones

    per_kv = QUERY_HEADS // KEY_VALUE_HEADS

    def attend(b, hide):
        start = pl.multiple_of(b * BLK, BLK)
        ahead = pl.ds(start, BLK)
        both = pl.ds(pl.multiple_of(start - BLK, BLK), 2 * BLK)

        def query_rows(h):
            source, row = (QA, h) if h < own_heads else (QB, h - own_heads)
            return source[row * HEAD_SIZE : (row + 1) * HEAD_SIZE, ahead]

        def attend_part(first_group, last_group):
            units = []
            for g in range(first_group, last_group):
                at_head = slice(g * HEAD_SIZE, (g + 1) * HEAD_SIZE)
                if hide is None:
                    key_part = KB[both, at_head]
                    value_part = VT[at_head, both]
                else:
                    key_part = jnp.concatenate([KH[:, at_head], KB[0:BLK, at_head]], axis=0)
                    value_part = jnp.concatenate([VH[at_head, :], VT[at_head, 0:BLK]], axis=1)
                for h in range(g * per_kv, (g + 1) * per_kv, 2):
                    query_part = jnp.concatenate(
                        [query_rows(h), query_rows(h + 1)], axis=1
                    )
                    sink = jnp.concatenate([SK[h : h + 1, :], SK[h + 1 : h + 2, :]], axis=1)
                    score = jnp.dot(key_part, query_part, preferred_element_type=F32)
                    units.append((h, score, value_part, sink))
            results = []
            for h, score, value_part, sink in units:
                before = score[:BLK]
                if hide is not None:
                    before = before + hide
                merged = jnp.where(older, before, score[BLK:])
                row_max = jnp.maximum(jnp.max(merged, axis=0, keepdims=True), sink)
                weights = jnp.exp(merged - row_max)
                weight_sum = jnp.sum(weights, axis=0, keepdims=True) + jnp.exp(sink - row_max)
                spread = jnp.concatenate(
                    [
                        jnp.where(older, weights, 0.0).astype(BF16),
                        jnp.where(older, 0.0, weights).astype(BF16),
                    ],
                    axis=0,
                )
                mixed = jnp.dot(value_part, spread, preferred_element_type=F32)
                mixed = mixed * (1.0 / weight_sum)
                stacked = jnp.concatenate([mixed[:, :BLK], mixed[:, BLK:]], axis=0).astype(BF16)
                results.append((h, stacked.T, row_max + jnp.log(weight_sum)))
            for h, out, logs in results:
                LS[h : h + 1, ahead] = logs[:, :BLK]
                LS[h + 1 : h + 2, ahead] = logs[:, BLK:]
                column = pw + lax.rem(tp * half_q + h * HEAD_SIZE, qw)
                ACT[ahead, pl.ds(pl.multiple_of(column, 128), 2 * HEAD_SIZE)] = out

        for g in range(0, KEY_VALUE_HEADS, PART):
            attend_part(g, g + PART)

    @pl.loop(1, blocks)
    def _(b):
        attend(b, None)

    @pl.when(jnp.logical_not(first))
    def _():
        for copy in halo_copies:
            copy.wait_recv()

    attend(0, jnp.where(first, -jnp.inf, 0.0).astype(F32))

    mine = pl.ds(pl.multiple_of(tp * rows, 128), rows)
    log_swap = pltpu.make_async_remote_copy(
        src_ref=LS.at[own_heads : 2 * own_heads, :],
        dst_ref=LSR.at[:, mine],
        send_sem=lsend_sem,
        recv_sem=lrecv_sem,
        device_id={"tp": 1 - tp},
        device_id_type=MESH,
    )
    log_swap.start()
    LSR[:, mine] = LS[0:own_heads, :]

    EARLIER[...] = jnp.zeros_like(EARLIER)

    @pl.loop(0, count)
    def _(source):
        @pl.when(source < me)
        def _():
            pltpu.make_async_remote_copy(
                src_ref=TOT,
                dst_ref=RECV.at[source],
                send_sem=tsend_sem.at[0],
                recv_sem=trecv_sem.at[source],
                device_id=mesh_id(source),
                device_id_type=MESH,
            ).wait_recv()
            EARLIER[...] += RECV[source]

    local_row = lax.broadcasted_iota(jnp.int32, (BLK, 128), 0)

    def pool(b, opening):
        start = pl.multiple_of(b * BLK, BLK)
        seen = (me * rows + b * BLK + 1 + local_row).astype(F32)
        per_seen = 1.0 / seen
        per_seen = jnp.concatenate([per_seen, per_seen], axis=1)
        sums, befores, carries, outs = [], [], [], []
        for j in range(GROUPS):
            side, at_group = j // 2, slice((j % 2) * GDIM, (j % 2 + 1) * GDIM)
            held = PA if side == 0 else PB
            if opening:
                source = jnp.concatenate([PH[side, :, at_group], held[0:BLK, at_group]], axis=0)
            else:
                source = held[pl.ds(pl.multiple_of(start - HALO, HALO), span), at_group]
            sums.append(jnp.dot(BAND[j], source, preferred_element_type=F32))
            befores.append(EARLIER[pl.ds(tp if side == 0 else 1 - tp, 1), 0, at_group])
        for j in range(GROUPS):
            window_mean = sums[j][:BLK]
            if opening:
                reach = reaches[j].astype(F32)
                fewer = reach / jnp.minimum(seen, reach)
                window_mean = window_mean * jnp.concatenate([fewer, fewer], axis=1)
            prefix = sums[j][BLK:] + befores[j]
            carries.append(prefix[BLK - 1 : BLK, :])
            pooled = (window_mean - prefix * per_seen).astype(BF16)
            outs.append(jnp.dot(pooled, WG[j], preferred_element_type=F32).astype(BF16))
        for j in range(GROUPS):
            side, at_group = j // 2, slice((j % 2) * GDIM, (j % 2 + 1) * GDIM)
            EARLIER[pl.ds(tp if side == 0 else 1 - tp, 1), 0, at_group] = carries[j]
            column = pl.multiple_of(groups[j] * GDIM, GDIM)
            ACT[pl.ds(start, BLK), pl.ds(column, GDIM)] = outs[j]

    pool(0, True)

    @pl.loop(1, blocks)
    def _(b):
        pool(b, False)

    log_swap.wait()

    @pl.when(jnp.logical_not(last))
    def _():
        for copy in halo_copies:
            copy.wait_send()

    @pl.loop(1, count)
    def _(step):
        @pl.when(me + step < count)
        def _():
            total_copy(me + step, step).wait_send()


def output_kernel(acts, w_out, logs, mixed_out, logs_out, MIXED, out_sem, log_sem):
    rows, width = MIXED.shape
    n_cols = 512
    log_copy = pltpu.make_async_copy(logs, logs_out, log_sem)
    log_copy.start()

    def out_copy(n):
        at = pl.ds(pl.multiple_of(n * n_cols, n_cols), n_cols)
        return pltpu.make_async_copy(MIXED.at[:, at], mixed_out.at[:, at], out_sem.at[n])

    @pl.loop(0, width // n_cols)
    def _(n):
        column = pl.ds(pl.multiple_of(n * n_cols, n_cols), n_cols)
        MIXED[:, column] = jnp.dot(
            acts[...], w_out[:, column], preferred_element_type=F32
        ).astype(BF16)
        out_copy(n).start()

    @pl.loop(0, width // n_cols)
    def _(n):
        out_copy(n).wait()

    log_copy.wait()


def body(sp_count, tokens, norm_gain, w_query, w_key, w_value, w_pool, w_group, w_out, sinks):
    token_rows = tokens[0]
    both_rows, width = token_rows.shape
    rows = both_rows // 2
    pw, qw, kw = 2 * w_pool.shape[1], 2 * w_query.shape[1], 2 * w_key.shape[1]
    count = sp_count * 2
    blocks = rows // BLK
    hbm = pl.BlockSpec(memory_space=pltpu.HBM)
    vmem = pl.BlockSpec(memory_space=pltpu.VMEM)
    dma = pltpu.SemaphoreType.DMA
    arguments = (
        token_rows,
        norm_gain[None, :],
        w_query,
        w_key,
        w_value,
        w_pool,
        w_group,
        sinks,
    )
    projected = pl.pallas_call(
        project_kernel,
        out_shape=(
            jax.ShapeDtypeStruct((rows, width), BF16),
            jax.ShapeDtypeStruct((width, pw // 2), BF16),
            jax.ShapeDtypeStruct((width, qw // 2), BF16),
            jax.ShapeDtypeStruct((width, 2 * kw), BF16),
            jax.ShapeDtypeStruct((GROUPS, GDIM, GDIM), BF16),
            jax.ShapeDtypeStruct((QUERY_HEADS, 128), F32),
            jax.ShapeDtypeStruct((rows, pw // 2), BF16),
            jax.ShapeDtypeStruct((qw // 2, rows), BF16),
            jax.ShapeDtypeStruct((1, pw // 2), F32),
        ),
        in_specs=[hbm] * 8,
        out_specs=(vmem,) * 9,
        scratch_shapes=[
            pltpu.VMEM((1, width), F32),
            pltpu.SMEM((QUERY_HEADS // 2,), F32),
            pltpu.VMEM((width, pw // 2), BF16),
            pltpu.VMEM((width, qw // 2), BF16),
            dma((blocks,)),
            dma((5,)),
            dma((2,)),
            dma((6,)),
            dma((6,)),
        ],
        compiler_params=pltpu.CompilerParams(
            collective_id=0, has_side_effects=True, vmem_limit_bytes=24 * 2**20
        ),
        name="project",
    )(*(pltpu.with_memory_space_constraint(array, pltpu.HBM) for array in arguments))

    acts, logs = pl.pallas_call(
        functools.partial(mixer_kernel, sp_count),
        out_shape=(
            jax.ShapeDtypeStruct((rows, pw + qw), BF16),
            jax.ShapeDtypeStruct((QUERY_HEADS // 2, both_rows), F32),
        ),
        in_specs=[vmem] * 9,
        out_specs=(vmem, vmem),
        scratch_shapes=[
            pltpu.VMEM((rows, pw // 2), BF16),
            pltpu.VMEM((qw // 2, rows), BF16),
            pltpu.VMEM((rows, kw), BF16),
            pltpu.VMEM((kw, rows), BF16),
            pltpu.VMEM((2, HALO, pw // 2), BF16),
            pltpu.VMEM((BLK, kw), BF16),
            pltpu.VMEM((kw, BLK), BF16),
            pltpu.VMEM((QUERY_HEADS, rows), F32),
            pltpu.VMEM((2, 1, pw // 2), F32),
            pltpu.VMEM((2, 1, pw // 2), F32),
            pltpu.VMEM((count, 2, 1, pw // 2), F32),
            pltpu.VMEM((GROUPS, 2 * BLK, HALO + BLK), BF16),
            dma((6,)),
            dma((6,)),
            dma((count,)),
            dma((count,)),
            dma,
            dma,
        ],
        compiler_params=pltpu.CompilerParams(
            collective_id=1, has_side_effects=True, vmem_limit_bytes=28 * 2**20
        ),
        name="mixers",
    )(*projected)

    n_cols = 512
    mixed, log_sums = pl.pallas_call(
        output_kernel,
        out_shape=(
            jax.ShapeDtypeStruct((rows, w_out.shape[1]), BF16),
            jax.ShapeDtypeStruct((QUERY_HEADS // 2, both_rows), F32),
        ),
        in_specs=[vmem, vmem, vmem],
        out_specs=(hbm, hbm),
        scratch_shapes=[
            pltpu.VMEM((rows, w_out.shape[1]), BF16),
            dma((w_out.shape[1] // n_cols,)),
            dma,
        ],
        compiler_params=pltpu.CompilerParams(vmem_limit_bytes=20 * 2**20),
        name="output",
    )(acts, w_out, logs)
    return mixed[None], log_sums[None]


def solution(mesh):
    return jax.shard_map(
        functools.partial(body, mesh.shape["sp"]),
        mesh=mesh,
        in_specs=(
            P("fs", "sp", None),
            P(),
            P(None, "tp"),
            P(None, "tp"),
            P(None, "tp"),
            P(None, "tp"),
            P("tp", None, None),
            P(),
            P("tp"),
        ),
        out_specs=(P("fs", ("sp", "tp"), None), P("fs", "tp", "sp")),
        check_vma=False,
    )
```

profile of v0, /device:TPU:1, one launch (start us, length us, event | category | flops | bytes accessed | tf_op | source)
XLA Modules:
  0.0 41.6 jit_solution(9045611548175603263)
XLA Ops:
  0.6 11.2 %project.1 = (bf16[1024,2048]{1,0:T(8,128)(2,1)S(1)}, bf16[2048,512]{1,0:T(8,128)(2,1)S(1)}, bf16[2048,512]{1,0:T(8,128)(2,1)S(1)}, bf16[2048,512]{1,0:T(8,128)(...) custom-call(bf16[2048,2048]{1,0:T(8,128)(2,1)} %bitcast.4, ...), custom_call_target="tpu_custom_call" | custom-call | tf_op jit(solution)/shard_map/project/pallas_call | solution.py:488
  11.8 0.0 copy-start
  11.8 19.3 %mixers.1 = (bf16[1024,2048]{1,0:T(8,128)(2,1)S(1)}, f32[8,2048]{1,0:T(8,128)S(1)}) custom-call(bf16[1024,2048]{1,0:T(8,128)(2,1)S(1)} %get-tuple-element.15.X, bf16[2048,512]{1,0:T(8,128)(2,1)S(1)} %get-tuple-element.16.WP, bf16[2048,512]{1,0:T(8,128)(2,1)S(1)} %get-tuple-element.17.WQ, bf16[2048,512]{1,0:T(8,128)(2,1)S(1)} %get-tuple-element.18.WKV, ...), custom_call_target="tpu_custom_call" | custom-call | tf_op jit(solution)/shard_map/mixers/pallas_call | solution.py:520
  31.2 0.0 copy-done
  31.2 10.4 %output.1 = (bf16[1024,2048]{1,0:T(8,128)(2,1)}, f32[8,2048]{1,0:T(8,128)}) custom-call(bf16[1024,2048]{1,0:T(8,128)(2,1)S(1)} %get-tuple-element.24.acts, bf16[2048,2048]{1,0:T(8,128)(2,1)S(1)} %copy-done, f32[8,2048]{1,0:T(8,128)S(1)} %get-tuple-element.25.logs), custom_call_target="tpu_custom_call" | custom-call | tf_op jit(solution)/shard_map/output/pallas_call | solution.py:555
Async XLA Ops:
  11.8 19.4 %copy-start = (bf16[2048,2048]{1,0:T(8,128)(2,1)S(1)}, bf16[2048,2048]{1,0:T(8,128)(2,1)}, u32[]{:S(2)}) copy-start(bf16[2048,2048]{1,0:T(8,128)(2,1)} %w_out.1) | copy-start | bytes 25165828
where the time goes:
time: 41.7 us; the launch traced here: 41.6 us
  Pallas kernels  40.9 us (98%)
  between operations  0.66 us (2%)
    pallas_call x1, Pallas kernels, body(): pl.pallas_call(functools.partial(mixer_kernel, sp_count), out_shape=(jax....  19.3 us
    pallas_call x1, Pallas kernels, body(): pl.pallas_call(project_kernel, out_shape=(jax.ShapeDtypeStruct((rows, wid...  11.2 us
    pallas_call x1, Pallas kernels, body(): pl.pallas_call(output_kernel, out_shape=(jax.ShapeDtypeStruct((rows, w_ou...  10.4 us

commit v1 on v0

v1 whole, which is shorter than its diff:
```python
import functools

import jax
import jax.numpy as jnp
from jax import lax
from jax.experimental import pallas as pl
from jax.experimental.pallas import tpu as pltpu
from jax.sharding import PartitionSpec as P

HEAD_SIZE = 64
GROUPS = 4
GDIM = 256
WINDOW_KEYS = 128
QUERY_HEADS = 16
KEY_VALUE_HEADS = 4
LN_EPS = 1e-05

BLK = 128
HALO = 16
TILE = 256
F32, BF16 = jnp.float32, jnp.bfloat16


MESH = pl.DeviceIdType.MESH
NORM_ROWS = 128
NORM_TILE = 256
STEPS = (512,)
AHEAD = 6


def project_kernel(
    tok,
    gain,
    w_query,
    w_key,
    w_value,
    w_pool,
    w_group,
    sinks,
    X,
    WP,
    WQ,
    WKV,
    WG,
    SK,
    PA,
    QA,
    KA,
    VA,
    TA,
    GAIN,
    GAINS,
    SINK,
    WPO,
    WQO,
    WKVO,
    x_sem,
    w_sem,
    small_sem,
    send_sem,
    recv_sem,
):
    rows, width = X.shape
    blocks = rows // BLK
    half_p, half_q, half_k = PA.shape[1], QA.shape[0], KA.shape[1]
    own_heads = QUERY_HEADS // 2
    tp = lax.axis_index("tp")
    peer = {"tp": 1 - tp}

    barrier = pltpu.get_barrier_semaphore()
    pl.semaphore_signal(barrier, inc=1, device_id=peer, device_id_type=MESH)

    small = [
        pltpu.make_async_copy(gain, GAIN, small_sem.at[0]),
        pltpu.make_async_copy(sinks, SINK, small_sem.at[1]),
    ]
    for copy in small:
        copy.start()

    def x_copy(b):
        return pltpu.make_async_copy(
            tok.at[pl.ds(pl.multiple_of(tp * rows + b * BLK, BLK), BLK), :],
            X.at[b * BLK : (b + 1) * BLK, :],
            x_sem.at[b],
        )

    for b in range(blocks):
        x_copy(b).start()

    pl.semaphore_wait(barrier, 1)
    sends = [
        pltpu.make_async_remote_copy(
            src_ref=src,
            dst_ref=dst,
            send_sem=send_sem.at[i],
            recv_sem=recv_sem.at[i],
            device_id=peer,
            device_id_type=MESH,
        )
        for i, (src, dst) in enumerate(
            (
                (w_pool, WP),
                (w_key, WKV.at[:, 0:half_k]),
                (w_value, WKV.at[:, half_k : 2 * half_k]),
                (w_query, WQ),
                (w_group, WG.at[GROUPS // 2 : GROUPS]),
                (SK.at[0:own_heads], SK.at[own_heads : 2 * own_heads]),
            )
        )
    ]
    for copy in sends[:5]:
        copy.start()

    own = [
        pltpu.make_async_copy(src, dst, w_sem.at[i])
        for i, (src, dst) in enumerate(
            (
                (w_pool, WPO),
                (w_query, WQO),
                (w_key, WKVO.at[:, 0:half_k]),
                (w_value, WKVO.at[:, half_k : 2 * half_k]),
                (w_group, WG.at[0 : GROUPS // 2]),
            )
        )
    ]
    for copy in own:
        copy.start()

    for copy in small:
        copy.wait()
    row_of = lax.broadcasted_iota(jnp.int32, (own_heads, 128), 0)
    sink_block = jnp.zeros((own_heads, 128), F32)
    for h in range(own_heads):
        sink_block = jnp.where(row_of == h, SINK[h], sink_block)
    SK[0:own_heads, :] = sink_block

    GAINS[...] = jnp.broadcast_to(GAIN[...], GAINS.shape)

    def normalized(row):
        values = X[row : row + NORM_ROWS, :].astype(F32)
        mean = jnp.sum(values, axis=-1, keepdims=True) * (1.0 / width)
        centered = values - mean
        variance = jnp.sum(centered * centered, axis=-1, keepdims=True) * (1.0 / width)
        scaled = (centered * lax.rsqrt(variance + LN_EPS)).reshape(-1, 8, width)
        return (scaled * GAINS[...][None]).reshape(NORM_ROWS, width).astype(BF16)

    def project(first_row, last_row, normed_to):
        at = slice(first_row, last_row)
        todo = list(range(last_row, normed_to, NORM_ROWS))
        slots = (half_p + half_q) // NORM_TILE
        following, pools, queries = [], [], []
        rows_in = X[at, :]

        def norm_some(slot):
            for row in todo[len(todo) * slot // slots : len(todo) * (slot + 1) // slots]:
                following.append((row, normalized(row)))

        for n in range(0, half_p, NORM_TILE):
            pools.append(jnp.dot(rows_in, WPO[:, n : n + NORM_TILE], preferred_element_type=F32))
            norm_some(n // NORM_TILE)
        for n in range(0, half_q, NORM_TILE):
            queries.append(jnp.dot(rows_in, WQO[:, n : n + NORM_TILE], preferred_element_type=F32))
            norm_some((half_p + n) // NORM_TILE)
        both = jnp.dot(rows_in, WKVO[...], preferred_element_type=F32).astype(BF16)
        for row, block in following:
            X[row : row + NORM_ROWS, :] = block
        for index, pool in enumerate(pools):
            columns = slice(index * NORM_TILE, (index + 1) * NORM_TILE)
            rounded = pool.astype(BF16)
            PA[at, columns] = rounded
            total = jnp.sum(rounded.astype(F32), axis=0, keepdims=True)
            TA[:, columns] = total if first_row == 0 else TA[:, columns] + total
        for index, query in enumerate(queries):
            at_rows = slice(index * NORM_TILE, (index + 1) * NORM_TILE)
            QA[at_rows, at] = (query * (HEAD_SIZE**-0.5)).astype(BF16).T
        KA[at, :] = both[:, :half_k]
        VA[:, at] = both[:, half_k:].T

    for row in range(0, STEPS[0], NORM_ROWS):
        x_copy(row // BLK).wait()
        X[row : row + NORM_ROWS, :] = normalized(row)
    for b in range(STEPS[0] // BLK, blocks):
        x_copy(b).wait()
    sends[5].start()
    for copy in own:
        copy.wait()
    bounds = (0, *STEPS, rows, rows)
    for step in range(len(bounds) - 2):
        project(*bounds[step : step + 3])

    for copy in sends:
        copy.wait()


def mixer_kernel(
    sp_count,
    X,
    WP,
    WQ,
    WKV,
    WG,
    SK,
    PA,
    QA,
    KA,
    VA,
    TA,
    w_out,
    ACT,
    LSR,
    WO,
    PB,
    QB,
    KB,
    VB,
    PH,
    KH,
    VH,
    LS,
    TOT,
    EARLIER,
    RECV,
    KEEP,
    BAND,
    hsend_sem,
    hrecv_sem,
    tsend_sem,
    trecv_sem,
    lsend_sem,
    lrecv_sem,
    out_sem,
):
    rows, half_k = KB.shape
    half_p, half_q = PA.shape[1], QA.shape[0]
    pw, qw = 2 * half_p, 2 * half_q
    blocks = rows // BLK
    sp, tp = lax.axis_index("sp"), lax.axis_index("tp")
    me = sp * 2 + tp
    count = sp_count * 2
    own_heads = QUERY_HEADS // 2
    first, last = me == 0, me == count - 1

    out_copy = pltpu.make_async_copy(w_out, WO, out_sem)
    out_copy.start()

    barrier = pltpu.get_barrier_semaphore()

    def arrive(device):
        pl.semaphore_signal(barrier, inc=1, device_id=device, device_id_type=MESH)

    arrive({"tp": 1 - tp})
    for distance in range(1, sp_count):
        place = sp + distance
        place = jnp.where(place >= sp_count, place - sp_count, place)
        for core in range(2):
            arrive({"sp": place, "tp": core})

    @pl.when(first)
    def _():
        PH[...] = jnp.zeros_like(PH)
        KH[...] = jnp.zeros_like(KH)
        VH[...] = jnp.zeros_like(VH)

    tile = jnp.dot(X[...], WP[...], preferred_element_type=F32).astype(BF16)
    PB[...] = tile
    TOT[pl.ds(tp, 1), 0] = TA[...]
    TOT[pl.ds(1 - tp, 1), 0] = jnp.sum(tile.astype(F32), axis=0, keepdims=True)
    tile = jnp.dot(X[...], WKV[...], preferred_element_type=F32).astype(BF16)
    KB[...] = tile[:, :half_k]
    VB[...] = tile[:, half_k:].T
    tile = jnp.dot(X[...], WQ[...], preferred_element_type=F32) * (HEAD_SIZE**-0.5)
    QB[...] = tile.astype(BF16).T

    tail = slice(rows - BLK, rows)
    following = lax.rem(sp + tp, sp_count)
    halo_copies = [
        pltpu.make_async_remote_copy(
            src_ref=src,
            dst_ref=dst,
            send_sem=hsend_sem.at[i],
            recv_sem=hrecv_sem.at[i],
            device_id={"sp": following, "tp": 1 - tp},
            device_id_type=MESH,
        )
        for i, (src, dst) in enumerate(
            (
                (KA.at[tail, :], KH.at[1]),
                (KB.at[tail, :], KH.at[0]),
                (VA.at[:, tail], VH.at[1]),
                (VB.at[:, tail], VH.at[0]),
                (PA.at[rows - HALO : rows], PH.at[1]),
                (PB.at[rows - HALO : rows], PH.at[0]),
            )
        )
    ]

    def total_copy(place, core, source):
        return pltpu.make_async_remote_copy(
            src_ref=TOT,
            dst_ref=RECV.at[source],
            send_sem=tsend_sem.at[place * 2 + core],
            recv_sem=trecv_sem.at[source],
            device_id={"sp": place, "tp": core},
            device_id_type=MESH,
        )

    def for_later(act):
        @pl.when(tp == 0)
        def _():
            act(sp, 1)

        @pl.loop(sp + 1, sp_count)
        def _(place):
            act(place, 0)
            act(place, 1)

    pl.semaphore_wait(barrier, count - 1)

    @pl.when(jnp.logical_not(last))
    def _():
        for copy in halo_copies:
            copy.start()

    for_later(lambda place, core: total_copy(place, core, me).start())

    span = HALO + BLK
    pairs = 2 * BLK
    older = lax.broadcasted_iota(jnp.int32, (BLK, pairs), 0) > (
        lax.broadcasted_iota(jnp.int32, (BLK, pairs), 1) & (BLK - 1)
    )
    KEEP[0] = jnp.where(older, 1.0, 0.0).astype(BF16)
    KEEP[1] = jnp.where(older, 0.0, 1.0).astype(BF16)
    back = (
        lax.broadcasted_iota(jnp.int32, (BLK, span), 0)
        + HALO
        - lax.broadcasted_iota(jnp.int32, (BLK, span), 1)
    )
    in_block = lax.broadcasted_iota(jnp.int32, (BLK, span), 1) >= HALO
    prefix_ones = jnp.where((back >= 0) & in_block, 1.0, 0.0).astype(BF16)
    groups = [lax.rem(2 * tp + j, GROUPS) for j in range(GROUPS)]
    reaches = [jnp.left_shift(jnp.int32(2), group) for group in groups]
    for j, reach in enumerate(reaches):
        BAND[j, 0:BLK, :] = jnp.where(
            (back >= 0) & (back < reach), 1.0 / reach.astype(F32), 0.0
        ).astype(BF16)
        BAND[j, BLK : 2 * BLK, :] = prefix_ones

    per_kv = QUERY_HEADS // KEY_VALUE_HEADS

    def query_rows(h, ahead):
        source, row = (QA, h) if h < own_heads else (QB, h - own_heads)
        return source[row * HEAD_SIZE : (row + 1) * HEAD_SIZE, ahead]

    kv_side = KEY_VALUE_HEADS // 2

    def attend(*spec):
        units = []
        for b, hide in spec:
            start = pl.multiple_of(b * BLK, BLK)
            for h in range(0, QUERY_HEADS, 2):
                units.append((start, hide, h))
        parts = {}

        def ask(index):
            start, hide, h = units[index]
            ahead = pl.ds(start, BLK)
            both = pl.ds(pl.multiple_of(start - BLK, BLK), 2 * BLK)
            side, slot = divmod(h // per_kv, kv_side)
            keys, values = (KA, VA) if side == 0 else (KB, VB)
            at_head = slice(slot * HEAD_SIZE, (slot + 1) * HEAD_SIZE)
            if hide is None:
                key_part, value_part = keys[both, at_head], values[at_head, both]
            else:
                key_part = jnp.concatenate([KH[side, :, at_head], keys[0:BLK, at_head]], axis=0)
                value_part = jnp.concatenate([VH[side, at_head, :], values[at_head, 0:BLK]], axis=1)
            query_part = jnp.concatenate([query_rows(h, ahead), query_rows(h + 1, ahead)], axis=1)
            sink = jnp.concatenate([SK[h : h + 1, :], SK[h + 1 : h + 2, :]], axis=1)
            score = jnp.dot(key_part, query_part, preferred_element_type=F32)
            parts[index] = (ahead, hide, h, score, value_part, sink)

        for index in range(min(AHEAD, len(units))):
            ask(index)
        results = []
        for index in range(len(units)):
            ahead, hide, h, score, value_part, sink = parts.pop(index)
            before = score[:BLK]
            if hide is not None:
                before = before + hide
            merged = jnp.where(older, before, score[BLK:])
            row_max = jnp.maximum(jnp.max(merged, axis=0, keepdims=True), sink)
            weights = jnp.exp(merged - row_max)
            weight_sum = jnp.sum(weights, axis=0, keepdims=True) + jnp.exp(sink - row_max)
            rounded = weights.astype(BF16)
            if index + AHEAD < len(units):
                ask(index + AHEAD)
            spread = jnp.concatenate([rounded * KEEP[0], rounded * KEEP[1]], axis=0)
            mixed = jnp.dot(value_part, spread, preferred_element_type=F32)
            mixed = mixed * (1.0 / weight_sum)
            stacked = jnp.concatenate([mixed[:, :BLK], mixed[:, BLK:]], axis=0).astype(BF16)
            results.append((ahead, h, stacked.T, row_max + jnp.log(weight_sum)))
        for ahead, h, out, logs in results:
            LS[h : h + 1, ahead] = logs[:, :BLK]
            LS[h + 1 : h + 2, ahead] = logs[:, BLK:]
            column = pw + lax.rem(tp * half_q + h * HEAD_SIZE, qw)
            ACT[ahead, pl.ds(pl.multiple_of(column, 128), 2 * HEAD_SIZE)] = out

    @pl.loop(1, blocks // 2)
    def _(b):
        attend((2 * b, None), (2 * b + 1, None))

    @pl.when(jnp.logical_not(first))
    def _():
        for copy in halo_copies:
            copy.wait_recv()

    attend((1, None), (0, jnp.where(first, -jnp.inf, 0.0).astype(F32)))

    mine = pl.ds(pl.multiple_of(tp * rows, 128), rows)
    log_swap = pltpu.make_async_remote_copy(
        src_ref=LS.at[own_heads : 2 * own_heads, :],
        dst_ref=LSR.at[:, mine],
        send_sem=lsend_sem,
        recv_sem=lrecv_sem,
        device_id={"tp": 1 - tp},
        device_id_type=MESH,
    )
    log_swap.start()
    LSR[:, mine] = LS[0:own_heads, :]

    @pl.loop(0, sp)
    def _(place):
        total_copy(place, 0, place * 2).wait_recv()
        total_copy(place, 1, place * 2 + 1).wait_recv()

    @pl.when(tp == 1)
    def _():
        total_copy(sp, 0, sp * 2).wait_recv()

    earlier = jnp.zeros(EARLIER.shape, F32)
    for source in range(count - 1):
        earlier += jnp.where(source < me, RECV[source], 0.0)
    EARLIER[...] = earlier

    local_row = lax.broadcasted_iota(jnp.int32, (BLK, 128), 0)

    def pool(*spec):
        units = []
        for b, opening in spec:
            start = pl.multiple_of(b * BLK, BLK)
            for j in range(GROUPS):
                side, at_group = j // 2, slice((j % 2) * GDIM, (j % 2 + 1) * GDIM)
                held = PA if side == 0 else PB
                if opening:
                    source = jnp.concatenate([PH[side, :, at_group], held[0:BLK, at_group]], axis=0)
                else:
                    source = held[pl.ds(pl.multiple_of(start - HALO, HALO), span), at_group]
                units.append(jnp.dot(BAND[j], source, preferred_element_type=F32))
        sides = [pl.ds(tp if j < 2 else 1 - tp, 1) for j in range(GROUPS)]
        carries = [
            EARLIER[sides[j], 0, (j % 2) * GDIM : (j % 2 + 1) * GDIM] for j in range(GROUPS)
        ]
        outs = []
        for (b, opening), sums in zip(spec, zip(*[iter(units)] * GROUPS)):
            seen = (me * rows + b * BLK + 1 + local_row).astype(F32)
            per_seen = 1.0 / seen
            per_seen = jnp.concatenate([per_seen, per_seen], axis=1)
            for j in range(GROUPS):
                window_mean = sums[j][:BLK]
                if opening:
                    reach = reaches[j].astype(F32)
                    fewer = reach / jnp.minimum(seen, reach)
                    window_mean = window_mean * jnp.concatenate([fewer, fewer], axis=1)
                prefix = sums[j][BLK:] + carries[j]
                carries[j] = prefix[BLK - 1 : BLK, :]
                pooled = (window_mean - prefix * per_seen).astype(BF16)
                out = jnp.dot(pooled, WG[j], preferred_element_type=F32).astype(BF16)
                outs.append((pl.ds(pl.multiple_of(b * BLK, BLK), BLK), groups[j], out))
        for j in range(GROUPS):
            EARLIER[sides[j], 0, (j % 2) * GDIM : (j % 2 + 1) * GDIM] = carries[j]
        for at, group, out in outs:
            ACT[at, pl.ds(pl.multiple_of(group * GDIM, GDIM), GDIM)] = out

    pool((0, True), (1, False))

    @pl.loop(1, blocks // 2)
    def _(b):
        pool((2 * b, False), (2 * b + 1, False))

    out_copy.wait()
    log_swap.wait()

    @pl.when(jnp.logical_not(last))
    def _():
        for copy in halo_copies:
            copy.wait_send()

    for_later(lambda place, core: total_copy(place, core, me).wait_send())


def output_kernel(acts, w_out, logs, mixed_out, logs_out, MIXED, out_sem, log_sem):
    rows, width = MIXED.shape
    n_cols = 512
    log_copy = pltpu.make_async_copy(logs, logs_out, log_sem)
    log_copy.start()

    def out_copy(n):
        at = pl.ds(pl.multiple_of(n * n_cols, n_cols), n_cols)
        return pltpu.make_async_copy(MIXED.at[:, at], mixed_out.at[:, at], out_sem.at[n])

    @pl.loop(0, width // n_cols)
    def _(n):
        column = pl.ds(pl.multiple_of(n * n_cols, n_cols), n_cols)
        MIXED[:, column] = jnp.dot(
            acts[...], w_out[:, column], preferred_element_type=F32
        ).astype(BF16)
        out_copy(n).start()

    @pl.loop(0, width // n_cols)
    def _(n):
        out_copy(n).wait()

    log_copy.wait()


def body(sp_count, tokens, norm_gain, w_query, w_key, w_value, w_pool, w_group, w_out, sinks):
    token_rows = tokens[0]
    both_rows, width = token_rows.shape
    rows = both_rows // 2
    pw, qw, kw = 2 * w_pool.shape[1], 2 * w_query.shape[1], 2 * w_key.shape[1]
    count = sp_count * 2
    blocks = rows // BLK
    hbm = pl.BlockSpec(memory_space=pltpu.HBM)
    vmem = pl.BlockSpec(memory_space=pltpu.VMEM)
    dma = pltpu.SemaphoreType.DMA
    arguments = (
        token_rows,
        norm_gain[None, :],
        w_query,
        w_key,
        w_value,
        w_pool,
        w_group,
        sinks,
    )
    projected = pl.pallas_call(
        project_kernel,
        out_shape=(
            jax.ShapeDtypeStruct((rows, width), BF16),
            jax.ShapeDtypeStruct((width, pw // 2), BF16),
            jax.ShapeDtypeStruct((width, qw // 2), BF16),
            jax.ShapeDtypeStruct((width, kw), BF16),
            jax.ShapeDtypeStruct((GROUPS, GDIM, GDIM), BF16),
            jax.ShapeDtypeStruct((QUERY_HEADS, 128), F32),
            jax.ShapeDtypeStruct((rows, pw // 2), BF16),
            jax.ShapeDtypeStruct((qw // 2, rows), BF16),
            jax.ShapeDtypeStruct((rows, kw // 2), BF16),
            jax.ShapeDtypeStruct((kw // 2, rows), BF16),
            jax.ShapeDtypeStruct((1, pw // 2), F32),
        ),
        in_specs=[hbm] * 8,
        out_specs=(vmem,) * 11,
        scratch_shapes=[
            pltpu.VMEM((1, width), F32),
            pltpu.VMEM((8, width), F32),
            pltpu.SMEM((QUERY_HEADS // 2,), F32),
            pltpu.VMEM((width, pw // 2), BF16),
            pltpu.VMEM((width, qw // 2), BF16),
            pltpu.VMEM((width, kw), BF16),
            dma((blocks,)),
            dma((5,)),
            dma((2,)),
            dma((6,)),
            dma((6,)),
        ],
        compiler_params=pltpu.CompilerParams(
            collective_id=0, has_side_effects=True, vmem_limit_bytes=20 * 2**20
        ),
        name="project",
    )(*(pltpu.with_memory_space_constraint(array, pltpu.HBM) for array in arguments))

    acts, logs, out_weights = pl.pallas_call(
        functools.partial(mixer_kernel, sp_count),
        out_shape=(
            jax.ShapeDtypeStruct((rows, pw + qw), BF16),
            jax.ShapeDtypeStruct((QUERY_HEADS // 2, both_rows), F32),
            jax.ShapeDtypeStruct(w_out.shape, BF16),
        ),
        in_specs=[vmem] * 11 + [hbm],
        out_specs=(vmem, vmem, vmem),
        scratch_shapes=[
            pltpu.VMEM((rows, pw // 2), BF16),
            pltpu.VMEM((qw // 2, rows), BF16),
            pltpu.VMEM((rows, kw // 2), BF16),
            pltpu.VMEM((kw // 2, rows), BF16),
            pltpu.VMEM((2, HALO, pw // 2), BF16),
            pltpu.VMEM((2, BLK, kw // 2), BF16),
            pltpu.VMEM((2, kw // 2, BLK), BF16),
            pltpu.VMEM((QUERY_HEADS, rows), F32),
            pltpu.VMEM((2, 1, pw // 2), F32),
            pltpu.VMEM((2, 1, pw // 2), F32),
            pltpu.VMEM((count, 2, 1, pw // 2), F32),
            pltpu.VMEM((2, BLK, 2 * BLK), BF16),
            pltpu.VMEM((GROUPS, 2 * BLK, HALO + BLK), BF16),
            dma((6,)),
            dma((6,)),
            dma((count,)),
            dma((count,)),
            dma,
            dma,
            dma,
        ],
        compiler_params=pltpu.CompilerParams(
            collective_id=1, has_side_effects=True, vmem_limit_bytes=20 * 2**20
        ),
        name="mixers",
    )(*projected, pltpu.with_memory_space_constraint(w_out, pltpu.HBM))

    n_cols = 512
    mixed, log_sums = pl.pallas_call(
        output_kernel,
        out_shape=(
            jax.ShapeDtypeStruct((rows, w_out.shape[1]), BF16),
            jax.ShapeDtypeStruct((QUERY_HEADS // 2, both_rows), F32),
        ),
        in_specs=[vmem, vmem, vmem],
        out_specs=(hbm, hbm),
        scratch_shapes=[
            pltpu.VMEM((rows, w_out.shape[1]), BF16),
            dma((w_out.shape[1] // n_cols,)),
            dma,
        ],
        compiler_params=pltpu.CompilerParams(vmem_limit_bytes=20 * 2**20),
        name="output",
    )(acts, out_weights, logs)
    return mixed[None], log_sums[None]


def solution(mesh):
    return jax.shard_map(
        functools.partial(body, mesh.shape["sp"]),
        mesh=mesh,
        in_specs=(
            P("fs", "sp", None),
            P(),
            P(None, "tp"),
            P(None, "tp"),
            P(None, "tp"),
            P(None, "tp"),
            P("tp", None, None),
            P(),
            P("tp"),
        ),
        out_specs=(P("fs", ("sp", "tp"), None), P("fs", "tp", "sp")),
        check_vma=False,
    )
```

time: 41.7 us -> 38.4 us (0.921)
  Pallas kernels: 40.9 us -> 37.4 us
    pallas_call x1, Pallas kernels: 19.3 us -> 16.4 us  [body(): pl.pallas_call(functools.partial(mixer_kernel, sp_count), out_shape=(jax....]
    pallas_call x1, Pallas kernels: 11.2 us -> 10.7 us  [body(): pl.pallas_call(project_kernel, out_shape=(jax.ShapeDtypeStruct((rows, wid...]
where the time goes in v1:
time: 38.4 us; the launch traced here: 38.2 us
  Pallas kernels  37.4 us (97%)
  between operations  0.81 us (2%)
    pallas_call x1, Pallas kernels, body(): pl.pallas_call(functools.partial(mixer_kernel, sp_count), out_shape=(jax....  16.4 us
    pallas_call x1, Pallas kernels, body(): pl.pallas_call(project_kernel, out_shape=(jax.ShapeDtypeStruct((rows, wid...  10.7 us
    pallas_call x1, Pallas kernels, body(): pl.pallas_call(output_kernel, out_shape=(jax.ShapeDtypeStruct((rows, w_ou...  10.4 us

profile of v1, /device:TPU:1, one launch (start us, length us, event | category | flops | bytes accessed | tf_op | source)
XLA Modules:
  0.0 38.2 jit_solution(6879549153654116888)
XLA Ops:
  0.6 10.7 %project.1 = (bf16[1024,2048]{1,0:T(8,128)(2,1)S(1)}, bf16[2048,512]{1,0:T(8,128)(2,1)S(1)}, bf16[2048,512]{1,0:T(8,128)(2,1)S(1)}, bf16[2048,256]{1,0:T(8,128)(...) custom-call(bf16[2048,2048]{1,0:T(8,128)(2,1)} %bitcast.4, ...), custom_call_target="tpu_custom_call" | custom-call | tf_op jit(solution)/shard_map/project/pallas_call | solution.py:545
  11.3 16.4 %mixers.1 = (bf16[1024,2048]{1,0:T(8,128)(2,1)S(1)}, f32[8,2048]{1,0:T(8,128)S(1)}, bf16[2048,2048]{1,0:T(8,128)(2,1)S(1)}) custom-call(bf16[1024,2048]{1,0:T(8,128)(2,1)S(1)} %get-tuple-element.18.X, bf16[2048,512]{1,0:T(8,128)(2,1)S(1)} %get-tuple-element.19.WP, bf16[2048,512]{1,0:T(8,128)(2,1)S(1)} %get-tuple-element.20.WQ, ...), custom_call_target="tpu_custom_call" | custom-call | tf_op jit(solution)/shard_map/mixers/pallas_call | solution.py:581
  27.7 10.4 %output.1 = (bf16[1024,2048]{1,0:T(8,128)(2,1)}, f32[8,2048]{1,0:T(8,128)}) custom-call(bf16[1024,2048]{1,0:T(8,128)(2,1)S(1)} %get-tuple-element.29.acts, bf16[2048,2048]{1,0:T(8,128)(2,1)S(1)} %get-tuple-element.30.w_out, f32[8,2048]{1,0:T(8,128)S(1)} %get-tuple-element.31.logs), custom_call_target="tpu_custom_call" | custom-call | tf_op jit(solution)/shard_map/output/pallas_call | solution.py:619

commit v2 on v1

--- a/solution.py
+++ b/solution.py
@@ -24,6 +24,9 @@
 MESH = pl.DeviceIdType.MESH
 NORM_ROWS = 128
 NORM_TILE = 256
+OUT_TILE = 512
+SEND_STEP = 2
+WG_INDEX, PA_INDEX = 4, 6
 STEPS = (512,)
 AHEAD = 6
 
@@ -206,22 +209,23 @@
     VA,
     TA,
     w_out,
-    ACT,
+    PART,
     LSR,
-    WO,
     PB,
+    PH,
+    EARLIER,
+    WOP,
+    ATT,
+    WOA,
     QB,
     KB,
     VB,
-    PH,
     KH,
     VH,
     LS,
     TOT,
-    EARLIER,
     RECV,
     KEEP,
-    BAND,
     hsend_sem,
     hrecv_sem,
     tsend_sem,
@@ -240,8 +244,12 @@
     own_heads = QUERY_HEADS // 2
     first, last = me == 0, me == count - 1
 
-    out_copy = pltpu.make_async_copy(w_out, WO, out_sem)
-    out_copy.start()
+    out_copies = [
+        pltpu.make_async_copy(w_out.at[pw : pw + qw], WOA, out_sem.at[0]),
+        pltpu.make_async_copy(w_out.at[0:pw], WOP, out_sem.at[1]),
+    ]
+    for copy in out_copies:
+        copy.start()
 
     barrier = pltpu.get_barrier_semaphore()
 
@@ -314,37 +322,22 @@
             act(place, 0)
             act(place, 1)
 
-    pl.semaphore_wait(barrier, count - 1)
-
-    @pl.when(jnp.logical_not(last))
-    def _():
-        for copy in halo_copies:
-            copy.start()
-
-    for_later(lambda place, core: total_copy(place, core, me).start())
-
-    span = HALO + BLK
+    def send_out():
+        pl.semaphore_wait(barrier, count - 1)
+
+        @pl.when(jnp.logical_not(last))
+        def _():
+            for copy in halo_copies:
+                copy.start()
+
+        for_later(lambda place, core: total_copy(place, core, me).start())
+
     pairs = 2 * BLK
     older = lax.broadcasted_iota(jnp.int32, (BLK, pairs), 0) > (
         lax.broadcasted_iota(jnp.int32, (BLK, pairs), 1) & (BLK - 1)
     )
     KEEP[0] = jnp.where(older, 1.0, 0.0).astype(BF16)
     KEEP[1] = jnp.where(older, 0.0, 1.0).astype(BF16)
-    back = (
-        lax.broadcasted_iota(jnp.int32, (BLK, span), 0)
-        + HALO
-        - lax.broadcasted_iota(jnp.int32, (BLK, span), 1)
-    )
-    in_block = lax.broadcasted_iota(jnp.int32, (BLK, span), 1) >= HALO
-    prefix_ones = jnp.where((back >= 0) & in_block, 1.0, 0.0).astype(BF16)
-    groups = [lax.rem(2 * tp + j, GROUPS) for j in range(GROUPS)]
-    reaches = [jnp.left_shift(jnp.int32(2), group) for group in groups]
-    for j, reach in enumerate(reaches):
-        BAND[j, 0:BLK, :] = jnp.where(
-            (back >= 0) & (back < reach), 1.0 / reach.astype(F32), 0.0
-        ).astype(BF16)
-        BAND[j, BLK : 2 * BLK, :] = prefix_ones
-
     per_kv = QUERY_HEADS // KEY_VALUE_HEADS
 
     def query_rows(h, ahead):
@@ -401,12 +394,26 @@
         for ahead, h, out, logs in results:
             LS[h : h + 1, ahead] = logs[:, :BLK]
             LS[h + 1 : h + 2, ahead] = logs[:, BLK:]
-            column = pw + lax.rem(tp * half_q + h * HEAD_SIZE, qw)
-            ACT[ahead, pl.ds(pl.multiple_of(column, 128), 2 * HEAD_SIZE)] = out
+            column = lax.rem(tp * half_q + h * HEAD_SIZE, qw)
+            ATT[ahead, pl.ds(pl.multiple_of(column, 128), 2 * HEAD_SIZE)] = out
+
+    def share(first_row, last_row):
+        for n in range(0, PART.shape[1], OUT_TILE):
+            PART[first_row:last_row, n : n + OUT_TILE] = jnp.dot(
+                ATT[first_row:last_row, :], WOA[:, n : n + OUT_TILE], preferred_element_type=F32
+            )
 
     @pl.loop(1, blocks // 2)
     def _(b):
+        @pl.when(b == SEND_STEP)
+        def _():
+            send_out()
+
         attend((2 * b, None), (2 * b + 1, None))
+
+    for copy in out_copies:
+        copy.wait()
+    share(2 * BLK, rows)
 
     @pl.when(jnp.logical_not(first))
     def _():
@@ -427,6 +434,8 @@
     log_swap.start()
     LSR[:, mine] = LS[0:own_heads, :]
 
+    share(0, 2 * BLK)
+
     @pl.loop(0, sp)
     def _(place):
         total_copy(place, 0, place * 2).wait_recv()
@@ -441,9 +450,70 @@
         earlier += jnp.where(source < me, RECV[source], 0.0)
     EARLIER[...] = earlier
 
+    log_swap.wait()
+
+    @pl.when(jnp.logical_not(last))
+    def _():
+        for copy in halo_copies:
+            copy.wait_send()
+
+    for_later(lambda place, core: total_copy(place, core, me).wait_send())
+
+
+def output_kernel(
+    PA,
+    PB,
+    PH,
+    before,
+    WG,
+    WOP,
+    PART,
+    logs,
+    mixed_out,
+    logs_out,
+    POOL,
+    MIXED,
+    EARLIER,
+    BAND,
+    out_sem,
+    log_sem,
+):
+    rows, half_p = PA.shape
+    width = MIXED.shape[1]
+    blocks = rows // BLK
+    tp = lax.axis_index("tp")
+    me = lax.axis_index("sp") * 2 + tp
+    log_copy = pltpu.make_async_copy(logs, logs_out, log_sem)
+    log_copy.start()
+
+    span = HALO + BLK
+    back = (
+        lax.broadcasted_iota(jnp.int32, (BLK, span), 0)
+        + HALO
+        - lax.broadcasted_iota(jnp.int32, (BLK, span), 1)
+    )
+    in_block = lax.broadcasted_iota(jnp.int32, (BLK, span), 1) >= HALO
+    prefix_ones = jnp.where((back >= 0) & in_block, 1.0, 0.0).astype(BF16)
+    groups = [lax.rem(2 * tp + j, GROUPS) for j in range(GROUPS)]
+    reaches = [jnp.left_shift(jnp.int32(2), group) for group in groups]
+    for j, reach in enumerate(reaches):
+        BAND[j, 0:BLK, :] = jnp.where(
+            (back >= 0) & (back < reach), 1.0 / reach.astype(F32), 0.0
+        ).astype(BF16)
+        BAND[j, BLK : 2 * BLK, :] = prefix_ones
+
+    EARLIER[...] = before[...]
     local_row = lax.broadcasted_iota(jnp.int32, (BLK, 128), 0)
-
-    def pool(*spec):
+    pair = 2 * BLK
+
+    def pair_rows(index):
+        return pl.ds(pl.multiple_of(index * pair, pair), pair)
+
+    def out_copy(index):
+        at = pair_rows(index)
+        return pltpu.make_async_copy(MIXED.at[at], mixed_out.at[at], out_sem.at[index])
+
+    def step(done, spec):
         units = []
         for b, opening in spec:
             start = pl.multiple_of(b * BLK, BLK)
@@ -454,71 +524,62 @@
                     source = jnp.concatenate([PH[side, :, at_group], held[0:BLK, at_group]], axis=0)
                 else:
                     source = held[pl.ds(pl.multiple_of(start - HALO, HALO), span), at_group]
-                units.append(jnp.dot(BAND[j], source, preferred_element_type=F32))
+                units.append((b, opening, j, source))
         sides = [pl.ds(tp if j < 2 else 1 - tp, 1) for j in range(GROUPS)]
         carries = [
             EARLIER[sides[j], 0, (j % 2) * GDIM : (j % 2 + 1) * GDIM] for j in range(GROUPS)
         ]
-        outs = []
-        for (b, opening), sums in zip(spec, zip(*[iter(units)] * GROUPS)):
+        sums = [
+            jnp.dot(BAND[j], source, preferred_element_type=F32) for b, opening, j, source in units
+        ]
+        rates = {}
+        for b, opening in spec:
             seen = (me * rows + b * BLK + 1 + local_row).astype(F32)
-            per_seen = 1.0 / seen
-            per_seen = jnp.concatenate([per_seen, per_seen], axis=1)
+            rates[id(b)] = (seen, 1.0 / seen)
+        outs, parts = [], []
+
+        def pool_unit(index):
+            b, opening, j, source = units[index]
+            seen, per_seen = rates[id(b)]
+            window_mean = sums[index][:BLK]
+            if opening:
+                reach = reaches[j].astype(F32)
+                fewer = reach / jnp.minimum(seen, reach)
+                window_mean = window_mean * jnp.concatenate([fewer, fewer], axis=1)
+            prefix = sums[index][BLK:] + carries[j]
+            carries[j] = prefix[BLK - 1 : BLK, :]
+            rate = jnp.concatenate([per_seen, per_seen], axis=1)
+            pooled = (window_mean - prefix * rate).astype(BF16)
+            out = jnp.dot(pooled, WG[j], preferred_element_type=F32).astype(BF16)
+            outs.append((pl.ds(pl.multiple_of(b * BLK, BLK), BLK), groups[j], out))
+
+        tiles = range(0, width, GDIM) if done is not None else ()
+        for index, n in enumerate(tiles):
+            ready = jnp.dot(POOL[pair_rows(done), :], WOP[:, n : n + GDIM], preferred_element_type=F32)
+            parts.append((n, (ready + PART[pair_rows(done), n : n + GDIM]).astype(BF16)))
+            if index < len(units):
+                pool_unit(index)
+        for index in range(len(tiles), len(units)):
+            pool_unit(index)
+        for n, part in parts:
+            MIXED[pair_rows(done), n : n + GDIM] = part
+        if units:
             for j in range(GROUPS):
-                window_mean = sums[j][:BLK]
-                if opening:
-                    reach = reaches[j].astype(F32)
-                    fewer = reach / jnp.minimum(seen, reach)
-                    window_mean = window_mean * jnp.concatenate([fewer, fewer], axis=1)
-                prefix = sums[j][BLK:] + carries[j]
-                carries[j] = prefix[BLK - 1 : BLK, :]
-                pooled = (window_mean - prefix * per_seen).astype(BF16)
-                out = jnp.dot(pooled, WG[j], preferred_element_type=F32).astype(BF16)
-                outs.append((pl.ds(pl.multiple_of(b * BLK, BLK), BLK), groups[j], out))
-        for j in range(GROUPS):
-            EARLIER[sides[j], 0, (j % 2) * GDIM : (j % 2 + 1) * GDIM] = carries[j]
+                EARLIER[sides[j], 0, (j % 2) * GDIM : (j % 2 + 1) * GDIM] = carries[j]
         for at, group, out in outs:
-            ACT[at, pl.ds(pl.multiple_of(group * GDIM, GDIM), GDIM)] = out
-
-    pool((0, True), (1, False))
+            POOL[at, pl.ds(pl.multiple_of(group * GDIM, GDIM), GDIM)] = out
+        if done is not None:
+            out_copy(done).start()
+
+    step(None, ((0, True), (1, False)))
 
     @pl.loop(1, blocks // 2)
-    def _(b):
-        pool((2 * b, False), (2 * b + 1, False))
-
-    out_copy.wait()
-    log_swap.wait()
-
-    @pl.when(jnp.logical_not(last))
-    def _():
-        for copy in halo_copies:
-            copy.wait_send()
-
-    for_later(lambda place, core: total_copy(place, core, me).wait_send())
-
-
-def output_kernel(acts, w_out, logs, mixed_out, logs_out, MIXED, out_sem, log_sem):
-    rows, width = MIXED.shape
-    n_cols = 512
-    log_copy = pltpu.make_async_copy(logs, logs_out, log_sem)
-    log_copy.start()
-
-    def out_copy(n):
-        at = pl.ds(pl.multiple_of(n * n_cols, n_cols), n_cols)
-        return pltpu.make_async_copy(MIXED.at[:, at], mixed_out.at[:, at], out_sem.at[n])
-
-    @pl.loop(0, width // n_cols)
-    def _(n):
-        column = pl.ds(pl.multiple_of(n * n_cols, n_cols), n_cols)
-        MIXED[:, column] = jnp.dot(
-            acts[...], w_out[:, column], preferred_element_type=F32
-        ).astype(BF16)
-        out_copy(n).start()
-
-    @pl.loop(0, width // n_cols)
-    def _(n):
-        out_copy(n).wait()
-
+    def _(index):
+        step(index - 1, ((2 * index, False), (2 * index + 1, False)))
+
+    step(blocks // 2 - 1, ())
+    for index in range(blocks // 2):
+        out_copy(index).wait()
     log_copy.wait()
 
 
@@ -578,36 +639,37 @@
         name="project",
     )(*(pltpu.with_memory_space_constraint(array, pltpu.HBM) for array in arguments))
 
-    acts, logs, out_weights = pl.pallas_call(
+    part, logs, other_pool, pool_halo, earlier, pool_weights = pl.pallas_call(
         functools.partial(mixer_kernel, sp_count),
         out_shape=(
-            jax.ShapeDtypeStruct((rows, pw + qw), BF16),
+            jax.ShapeDtypeStruct((rows, w_out.shape[1]), F32),
             jax.ShapeDtypeStruct((QUERY_HEADS // 2, both_rows), F32),
-            jax.ShapeDtypeStruct(w_out.shape, BF16),
+            jax.ShapeDtypeStruct((rows, pw // 2), BF16),
+            jax.ShapeDtypeStruct((2, HALO, pw // 2), BF16),
+            jax.ShapeDtypeStruct((2, 1, pw // 2), F32),
+            jax.ShapeDtypeStruct((pw, w_out.shape[1]), BF16),
         ),
         in_specs=[vmem] * 11 + [hbm],
-        out_specs=(vmem, vmem, vmem),
+        out_specs=(vmem,) * 6,
         scratch_shapes=[
-            pltpu.VMEM((rows, pw // 2), BF16),
+            pltpu.VMEM((rows, qw), BF16),
+            pltpu.VMEM((qw, w_out.shape[1]), BF16),
             pltpu.VMEM((qw // 2, rows), BF16),
             pltpu.VMEM((rows, kw // 2), BF16),
             pltpu.VMEM((kw // 2, rows), BF16),
-            pltpu.VMEM((2, HALO, pw // 2), BF16),
             pltpu.VMEM((2, BLK, kw // 2), BF16),
             pltpu.VMEM((2, kw // 2, BLK), BF16),
             pltpu.VMEM((QUERY_HEADS, rows), F32),
             pltpu.VMEM((2, 1, pw // 2), F32),
-            pltpu.VMEM((2, 1, pw // 2), F32),
             pltpu.VMEM((count, 2, 1, pw // 2), F32),
             pltpu.VMEM((2, BLK, 2 * BLK), BF16),
-            pltpu.VMEM((GROUPS, 2 * BLK, HALO + BLK), BF16),
             dma((6,)),
             dma((6,)),
             dma((count,)),
             dma((count,)),
             dma,
             dma,
-            dma,
+            dma((2,)),
         ],
         compiler_params=pltpu.CompilerParams(
             collective_id=1, has_side_effects=True, vmem_limit_bytes=20 * 2**20
@@ -615,23 +677,34 @@
         name="mixers",
     )(*projected, pltpu.with_memory_space_constraint(w_out, pltpu.HBM))
 
-    n_cols = 512
     mixed, log_sums = pl.pallas_call(
         output_kernel,
         out_shape=(
             jax.ShapeDtypeStruct((rows, w_out.shape[1]), BF16),
             jax.ShapeDtypeStruct((QUERY_HEADS // 2, both_rows), F32),
         ),
-        in_specs=[vmem, vmem, vmem],
+        in_specs=[vmem] * 8,
         out_specs=(hbm, hbm),
         scratch_shapes=[
+            pltpu.VMEM((rows, pw), BF16),
             pltpu.VMEM((rows, w_out.shape[1]), BF16),
-            dma((w_out.shape[1] // n_cols,)),
+            pltpu.VMEM((2, 1, pw // 2), F32),
+            pltpu.VMEM((GROUPS, 2 * BLK, HALO + BLK), BF16),
+            dma((blocks // 2,)),
             dma,
         ],
-        compiler_params=pltpu.CompilerParams(vmem_limit_bytes=20 * 2**20),
+        compiler_params=pltpu.CompilerParams(vmem_limit_bytes=24 * 2**20),
         name="output",
-    )(acts, out_weights, logs)
+    )(
+        projected[PA_INDEX],
+        other_pool,
+        pool_halo,
+        earlier,
+        projected[WG_INDEX],
+        pool_weights,
+        part,
+        logs,
+    )
     return mixed[None], log_sums[None]
 
 

time: 38.4 us -> 37.5 us (0.977)
  Pallas kernels: 37.4 us -> 36.5 us
    pallas_call x1, Pallas kernels: 10.4 us -> 7.99 us  [body(): pl.pallas_call(output_kernel, out_shape=(jax.ShapeDtypeStruct((rows, w_ou...]
    pallas_call x1, Pallas kernels: 16.4 us -> 17.8 us  [body(): pl.pallas_call(functools.partial(mixer_kernel, sp_count), out_shape=(jax....]
where the time goes in v2:
time: 37.5 us; the launch traced here: 37.4 us
  Pallas kernels  36.5 us (97%)
  between operations  0.83 us (2%)
    pallas_call x1, Pallas kernels, body(): pl.pallas_call(functools.partial(mixer_kernel, sp_count), out_shape=(jax....  17.8 us
    pallas_call x1, Pallas kernels, body(): pl.pallas_call(project_kernel, out_shape=(jax.ShapeDtypeStruct((rows, wid...  10.7 us
    pallas_call x1, Pallas kernels, body(): pl.pallas_call(output_kernel, out_shape=(jax.ShapeDtypeStruct((rows, w_ou...  7.99 us

profile of v2, /device:TPU:1, one launch (start us, length us, event | category | flops | bytes accessed | tf_op | source)
XLA Modules:
  0.0 37.4 jit_solution(10400941515804607269)
XLA Ops:
  0.6 10.7 %project.1 = (bf16[1024,2048]{1,0:T(8,128)(2,1)S(1)}, bf16[2048,512]{1,0:T(8,128)(2,1)S(1)}, bf16[2048,512]{1,0:T(8,128)(2,1)S(1)}, bf16[2048,256]{1,0:T(8,128)(...) custom-call(bf16[2048,2048]{1,0:T(8,128)(2,1)} %bitcast.4, ...), custom_call_target="tpu_custom_call" | custom-call | tf_op jit(solution)/shard_map/project/pallas_call | solution.py:606
  11.3 17.8 %mixers.1 = (f32[1024,2048]{1,0:T(8,128)S(1)}, f32[8,2048]{1,0:T(8,128)S(1)}, bf16[1024,512]{1,0:T(8,128)(2,1)S(1)}, bf16[2,16,512]{2,1,0:T(8,128)(2,1)S(1)}, f3...) custom-call(bf16[1024,2048]{1,0:T(8,128)(2,1)S(1)} %get-tuple-element.22.X, ...), custom_call_target="tpu_custom_call" | custom-call | tf_op jit(solution)/shard_map/mixers/pallas_call | solution.py:642
  29.2 8.0 %output.1 = (bf16[1024,2048]{1,0:T(8,128)(2,1)}, f32[8,2048]{1,0:T(8,128)}) custom-call(bf16[1024,512]{1,0:T(8,128)(2,1)S(1)} %get-tuple-element.21.PA, bf16[1024,512]{1,0:T(8,128)(2,1)S(1)} %get-tuple-element.32.PB, bf16[2,16,512]{2,1,0:T(8,128)(2,1)S(1)} %get-tuple-element.33.PH, f32[2,1,512]{2,1,0:T(1,128)S(1)} %get-tuple-element.34.before, ...), custom_call_target="tpu_custom_call" | custom-call | tf_op jit(solution)/shard_map/output/pallas_call | solution.py:680

commit v3 on v2

--- a/solution.py
+++ b/solution.py
@@ -25,10 +25,9 @@
 NORM_ROWS = 128
 NORM_TILE = 256
 OUT_TILE = 512
-SEND_STEP = 2
 WG_INDEX, PA_INDEX = 4, 6
 STEPS = (512,)
-AHEAD = 6
+AHEAD = 8
 
 
 def project_kernel(
@@ -346,7 +345,11 @@
 
     kv_side = KEY_VALUE_HEADS // 2
 
-    def attend(*spec):
+    def attend(*spec, done=None):
+        ready = []
+        if done is not None:
+            at = pl.ds(pl.multiple_of(done * 2 * BLK, 2 * BLK), 2 * BLK)
+            attended = ATT[at, :]
         units = []
         for b, hide in spec:
             start = pl.multiple_of(b * BLK, BLK)
@@ -376,6 +379,11 @@
         results = []
         for index in range(len(units)):
             ahead, hide, h, score, value_part, sink = parts.pop(index)
+            if done is not None and index % 2 == 0:
+                n = (index // 2) * GDIM
+                ready.append(
+                    jnp.dot(attended, WOA[:, n : n + GDIM], preferred_element_type=F32)
+                )
             before = score[:BLK]
             if hide is not None:
                 before = before + hide
@@ -391,6 +399,8 @@
             mixed = mixed * (1.0 / weight_sum)
             stacked = jnp.concatenate([mixed[:, :BLK], mixed[:, BLK:]], axis=0).astype(BF16)
             results.append((ahead, h, stacked.T, row_max + jnp.log(weight_sum)))
+        for n, part in enumerate(ready):
+            PART[at, n * GDIM : (n + 1) * GDIM] = part
         for ahead, h, out, logs in results:
             LS[h : h + 1, ahead] = logs[:, :BLK]
             LS[h + 1 : h + 2, ahead] = logs[:, BLK:]
@@ -403,24 +413,24 @@
                 ATT[first_row:last_row, :], WOA[:, n : n + OUT_TILE], preferred_element_type=F32
             )
 
-    @pl.loop(1, blocks // 2)
-    def _(b):
-        @pl.when(b == SEND_STEP)
-        def _():
-            send_out()
-
-        attend((2 * b, None), (2 * b + 1, None))
-
+    @pl.when(me >= 0)
+    def _():
+        attend((2, None), (3, None))
+
+    send_out()
     for copy in out_copies:
         copy.wait()
-    share(2 * BLK, rows)
+
+    @pl.loop(2, blocks // 2)
+    def _(b):
+        attend((2 * b, None), (2 * b + 1, None), done=b - 1)
 
     @pl.when(jnp.logical_not(first))
     def _():
         for copy in halo_copies:
             copy.wait_recv()
 
-    attend((1, None), (0, jnp.where(first, -jnp.inf, 0.0).astype(F32)))
+    attend((1, None), (0, jnp.where(first, -jnp.inf, 0.0).astype(F32)), done=blocks // 2 - 1)
 
     mine = pl.ds(pl.multiple_of(tp * rows, 128), rows)
     log_swap = pltpu.make_async_remote_copy(

time: 37.5 us -> 36.7 us (0.979)
  Pallas kernels: 36.5 us -> 35.6 us
    pallas_call x1, Pallas kernels: 17.8 us -> 16.9 us  [body(): pl.pallas_call(functools.partial(mixer_kernel, sp_count), out_shape=(jax....]
where the time goes in v3:
time: 36.7 us; the launch traced here: 36.4 us
  Pallas kernels  35.6 us (97%)
  between operations  0.81 us (2%)
    pallas_call x1, Pallas kernels, body(): pl.pallas_call(functools.partial(mixer_kernel, sp_count), out_shape=(jax....  16.9 us
    pallas_call x1, Pallas kernels, body(): pl.pallas_call(project_kernel, out_shape=(jax.ShapeDtypeStruct((rows, wid...  10.7 us
    pallas_call x1, Pallas kernels, body(): pl.pallas_call(output_kernel, out_shape=(jax.ShapeDtypeStruct((rows, w_ou...  7.99 us

profile of v3, /device:TPU:1, one launch (start us, length us, event | category | flops | bytes accessed | tf_op | source)
XLA Modules:
  0.0 36.4 jit_solution(3423119203876338597)
XLA Ops:
  0.6 10.7 %project.1 = (bf16[1024,2048]{1,0:T(8,128)(2,1)S(1)}, bf16[2048,512]{1,0:T(8,128)(2,1)S(1)}, bf16[2048,512]{1,0:T(8,128)(2,1)S(1)}, bf16[2048,256]{1,0:T(8,128)(...) custom-call(bf16[2048,2048]{1,0:T(8,128)(2,1)} %bitcast.4, ...), custom_call_target="tpu_custom_call" | custom-call | tf_op jit(solution)/shard_map/project/pallas_call | solution.py:616
  11.3 16.9 %mixers.1 = (f32[1024,2048]{1,0:T(8,128)S(1)}, f32[8,2048]{1,0:T(8,128)S(1)}, bf16[1024,512]{1,0:T(8,128)(2,1)S(1)}, bf16[2,16,512]{2,1,0:T(8,128)(2,1)S(1)}, f3...) custom-call(bf16[1024,2048]{1,0:T(8,128)(2,1)S(1)} %get-tuple-element.22.X, ...), custom_call_target="tpu_custom_call" | custom-call | tf_op jit(solution)/shard_map/mixers/pallas_call | solution.py:652
  28.3 8.0 %output.1 = (bf16[1024,2048]{1,0:T(8,128)(2,1)}, f32[8,2048]{1,0:T(8,128)}) custom-call(bf16[1024,512]{1,0:T(8,128)(2,1)S(1)} %get-tuple-element.21.PA, bf16[1024,512]{1,0:T(8,128)(2,1)S(1)} %get-tuple-element.32.PB, bf16[2,16,512]{2,1,0:T(8,128)(2,1)S(1)} %get-tuple-element.33.PH, f32[2,1,512]{2,1,0:T(1,128)S(1)} %get-tuple-element.34.before, ...), custom_call_target="tpu_custom_call" | custom-call | tf_op jit(solution)/shard_map/output/pallas_call | solution.py:690

commit v4 on v3

--- a/solution.py
+++ b/solution.py
@@ -26,7 +26,7 @@
 NORM_TILE = 256
 OUT_TILE = 512
 WG_INDEX, PA_INDEX = 4, 6
-STEPS = (512,)
+STEPS = (640,)
 AHEAD = 8
 
 
@@ -374,7 +374,8 @@
             score = jnp.dot(key_part, query_part, preferred_element_type=F32)
             parts[index] = (ahead, hide, h, score, value_part, sink)
 
-        for index in range(min(AHEAD, len(units))):
+        lead = AHEAD if done is None else AHEAD // 2
+        for index in range(min(lead, len(units))):
             ask(index)
         results = []
         for index in range(len(units)):
@@ -392,8 +393,8 @@
             weights = jnp.exp(merged - row_max)
             weight_sum = jnp.sum(weights, axis=0, keepdims=True) + jnp.exp(sink - row_max)
             rounded = weights.astype(BF16)
-            if index + AHEAD < len(units):
-                ask(index + AHEAD)
+            if index + lead < len(units):
+                ask(index + lead)
             spread = jnp.concatenate([rounded * KEEP[0], rounded * KEEP[1]], axis=0)
             mixed = jnp.dot(value_part, spread, preferred_element_type=F32)
             mixed = mixed * (1.0 / weight_sum)

time: 36.7 us -> 36.4 us (level)
  Pallas kernels: 35.6 us -> 35.2 us
where the time goes in v4:
time: 36.4 us; the launch traced here: 36 us
  Pallas kernels  35.2 us (97%)
  between operations  0.81 us (2%)
    pallas_call x1, Pallas kernels, body(): pl.pallas_call(functools.partial(mixer_kernel, sp_count), out_shape=(jax....  16.7 us
    pallas_call x1, Pallas kernels, body(): pl.pallas_call(project_kernel, out_shape=(jax.ShapeDtypeStruct((rows, wid...  10.5 us
    pallas_call x1, Pallas kernels, body(): pl.pallas_call(output_kernel, out_shape=(jax.ShapeDtypeStruct((rows, w_ou...  7.98 us

profile of v4, /device:TPU:1, one launch (start us, length us, event | category | flops | bytes accessed | tf_op | source)
XLA Modules:
  0.0 36.0 jit_solution(10492486500486879136)
XLA Ops:
  0.6 10.5 %project.1 = (bf16[1024,2048]{1,0:T(8,128)(2,1)S(1)}, bf16[2048,512]{1,0:T(8,128)(2,1)S(1)}, bf16[2048,512]{1,0:T(8,128)(2,1)S(1)}, bf16[2048,256]{1,0:T(8,128)(...) custom-call(bf16[2048,2048]{1,0:T(8,128)(2,1)} %bitcast.4, ...), custom_call_target="tpu_custom_call" | custom-call | tf_op jit(solution)/shard_map/project/pallas_call | solution.py:617
  11.2 16.7 %mixers.1 = (f32[1024,2048]{1,0:T(8,128)S(1)}, f32[8,2048]{1,0:T(8,128)S(1)}, bf16[1024,512]{1,0:T(8,128)(2,1)S(1)}, bf16[2,16,512]{2,1,0:T(8,128)(2,1)S(1)}, f3...) custom-call(bf16[1024,2048]{1,0:T(8,128)(2,1)S(1)} %get-tuple-element.22.X, ...), custom_call_target="tpu_custom_call" | custom-call | tf_op jit(solution)/shard_map/mixers/pallas_call | solution.py:653
  27.8 8.0 %output.1 = (bf16[1024,2048]{1,0:T(8,128)(2,1)}, f32[8,2048]{1,0:T(8,128)}) custom-call(bf16[1024,512]{1,0:T(8,128)(2,1)S(1)} %get-tuple-element.21.PA, bf16[1024,512]{1,0:T(8,128)(2,1)S(1)} %get-tuple-element.32.PB, bf16[2,16,512]{2,1,0:T(8,128)(2,1)S(1)} %get-tuple-element.33.PH, f32[2,1,512]{2,1,0:T(1,128)S(1)} %get-tuple-element.34.before, ...), custom_call_target="tpu_custom_call" | custom-call | tf_op jit(solution)/shard_map/output/pallas_call | solution.py:691

commit v5 on v4

--- a/solution.py
+++ b/solution.py
@@ -588,9 +588,24 @@
     def _(index):
         step(index - 1, ((2 * index, False), (2 * index + 1, False)))
 
-    step(blocks // 2 - 1, ())
-    for index in range(blocks // 2):
+    final = slice(rows - pair, rows)
+    cut = width * 3 // 4
+    last_copies = []
+    for part, columns in enumerate((slice(0, cut), slice(cut, width))):
+        ready = jnp.dot(POOL[final, :], WOP[:, columns], preferred_element_type=F32)
+        MIXED[final, columns] = (ready + PART[final, columns]).astype(BF16)
+        last_copies.append(
+            pltpu.make_async_copy(
+                MIXED.at[final, columns],
+                mixed_out.at[final, columns],
+                out_sem.at[blocks // 2 - 1 + part],
+            )
+        )
+        last_copies[part].start()
+    for index in range(blocks // 2 - 1):
         out_copy(index).wait()
+    for copy in last_copies:
+        copy.wait()
     log_copy.wait()
 
 
@@ -701,7 +716,7 @@
             pltpu.VMEM((rows, w_out.shape[1]), BF16),
             pltpu.VMEM((2, 1, pw // 2), F32),
             pltpu.VMEM((GROUPS, 2 * BLK, HALO + BLK), BF16),
-            dma((blocks // 2,)),
+            dma((blocks // 2 + 1,)),
             dma,
         ],
         compiler_params=pltpu.CompilerParams(vmem_limit_bytes=24 * 2**20),

time: 36.4 us -> 36.1 us (level)
  no operation moved by 1% of the time
where the time goes in v5:
time: 36.1 us; the launch traced here: 35.7 us
  Pallas kernels  34.9 us (97%)
  between operations  0.81 us (2%)
    pallas_call x1, Pallas kernels, body(): pl.pallas_call(functools.partial(mixer_kernel, sp_count), out_shape=(jax....  16.7 us
    pallas_call x1, Pallas kernels, body(): pl.pallas_call(project_kernel, out_shape=(jax.ShapeDtypeStruct((rows, wid...  10.5 us
    pallas_call x1, Pallas kernels, body(): pl.pallas_call(output_kernel, out_shape=(jax.ShapeDtypeStruct((rows, w_ou...  7.74 us

profile of v5, /device:TPU:1, one launch (start us, length us, event | category | flops | bytes accessed | tf_op | source)
XLA Modules:
  0.0 35.7 jit_solution(2945158686660566265)
XLA Ops:
  0.6 10.5 %project.1 = (bf16[1024,2048]{1,0:T(8,128)(2,1)S(1)}, bf16[2048,512]{1,0:T(8,128)(2,1)S(1)}, bf16[2048,512]{1,0:T(8,128)(2,1)S(1)}, bf16[2048,256]{1,0:T(8,128)(...) custom-call(bf16[2048,2048]{1,0:T(8,128)(2,1)} %bitcast.4, ...), custom_call_target="tpu_custom_call" | custom-call | tf_op jit(solution)/shard_map/project/pallas_call | solution.py:632
  11.2 16.7 %mixers.1 = (f32[1024,2048]{1,0:T(8,128)S(1)}, f32[8,2048]{1,0:T(8,128)S(1)}, bf16[1024,512]{1,0:T(8,128)(2,1)S(1)}, bf16[2,16,512]{2,1,0:T(8,128)(2,1)S(1)}, f3...) custom-call(bf16[1024,2048]{1,0:T(8,128)(2,1)S(1)} %get-tuple-element.22.X, ...), custom_call_target="tpu_custom_call" | custom-call | tf_op jit(solution)/shard_map/mixers/pallas_call | solution.py:668
  27.8 7.7 %output.1 = (bf16[1024,2048]{1,0:T(8,128)(2,1)}, f32[8,2048]{1,0:T(8,128)}) custom-call(bf16[1024,512]{1,0:T(8,128)(2,1)S(1)} %get-tuple-element.21.PA, bf16[1024,512]{1,0:T(8,128)(2,1)S(1)} %get-tuple-element.32.PB, bf16[2,16,512]{2,1,0:T(8,128)(2,1)S(1)} %get-tuple-element.33.PH, f32[2,1,512]{2,1,0:T(1,128)S(1)} %get-tuple-element.34.before, ...), custom_call_target="tpu_custom_call" | custom-call | tf_op jit(solution)/shard_map/output/pallas_call | solution.py:706
